TPU v7x, 32 devices: a whole 2x2x4 slice. The times are simulated.
32 devices in a mesh: fs: 4 (over y, x), tp: 8 (over z, core).
Axes of the slice: x: 2, y: 2, z: 4, core: 2. Of those that a mesh axis runs over, the one named last changes fastest.
Arguments:
- normed_inputs: bfloat16 [4096, 4096], P('fs', 'tp'), may hold values from -6 to 6
- query_upstream: bfloat16 [4096, 4096], P('fs', 'tp'), may hold values from -0.125 to 0.125
- key_upstream: bfloat16 [4096, 1024], P('fs', 'tp'), may hold values from -0.09375 to 0.09375
- head_outputs: bfloat16 [4096, 4096], P('fs', 'tp'), may hold values from -6 to 6
- branch_upstream: bfloat16 [4096, 4096], P('fs', 'tp'), may hold values from -0.125 to 0.125
- query_master: float32 [4096, 4096], P('fs', 'tp'), may hold values from -0.09375 to 0.09375
- key_master: float32 [4096, 1024], P('fs', 'tp'), may hold values from -0.09375 to 0.09375
- branch_master: float32 [4096, 4096], P('fs', 'tp'), may hold values from -0.09375 to 0.09375
- query_basis: bfloat16 [4096, 128], replicated, may hold values from -0.09375 to 0.09375
- key_basis: bfloat16 [4096, 128], replicated, may hold values from -0.09375 to 0.09375
- branch_basis: bfloat16 [4096, 128], replicated, may hold values from -0.09375 to 0.09375
- query_first: float32 [128, 4096], P(None, 'tp'), may hold values from -0.75 to 0.75
- query_second: float32 [128, 4096], P(None, 'tp'), may hold values from 0.001 to 0.02
- key_first: float32 [128, 1024], P(None, 'tp'), may hold values from -0.75 to 0.75
- key_second: float32 [128, 1024], P(None, 'tp'), may hold values from 0.001 to 0.02
- branch_first: float32 [4096, 128], P('fs'), may hold values from -0.75 to 0.75
- branch_second: float32 [4096, 128], P('fs'), may hold values from 0.001 to 0.02
Outputs:
- query_step: float32 [4096, 4096], P('fs', 'tp')
- key_step: float32 [4096, 1024], P('fs', 'tp')
- branch_step: float32 [4096, 4096], P('fs', 'tp')
- query_updated: float32 [4096, 4096], P('fs', 'tp')
- key_updated: float32 [4096, 1024], P('fs', 'tp')
- branch_updated: float32 [4096, 4096], P('fs', 'tp')
- query_copy: bfloat16 [4096, 4096], P(None, 'tp')
- key_copy: bfloat16 [4096, 1024], P(None, 'tp')
- branch_copy: bfloat16 [4096, 4096], P(None, 'tp')
- query_first_new: float32 [128, 4096], P(None, 'tp')
- query_second_new: float32 [128, 4096], P(None, 'tp')
- key_first_new: float32 [128, 1024], P(None, 'tp')
- key_second_new: float32 [128, 1024], P(None, 'tp')
- branch_first_new: float32 [4096, 128], P('fs')
- branch_second_new: float32 [4096, 128], P('fs')
All inputs are finite; a program needn't handle non-finite values.
Results may differ from a plain program's by a relative error of at most 0.001.
Values may be sent and summed in bfloat16 or wider, within the bound.
No kernel may reach another device: no remote copies, remote signals or barrier semaphores. Data moves between devices by JAX's collectives and lax.ppermute only.
A program may use at most 128 MiB of HBM per device.

v0:
```python
import jax
import jax.numpy as jnp
from jax import lax
from jax.sharding import PartitionSpec as P

LEARN = 0.02
BETA_ONE = 0.9
BETA_TWO = 0.95
ADAM_EPS = 1e-08
CLIP_RMS = 0.5


def moments(first, second, low, clip):
    scaled = clip * low
    first_new = BETA_ONE * first + (1.0 - BETA_ONE) * scaled
    second_new = BETA_TWO * second + (1.0 - BETA_TWO) * scaled * scaled
    return (first_new, second_new, first_new / (jnp.sqrt(second_new) + ADAM_EPS))


def over_tokens(left, right, precision=None):
    return lax.dot_general(
        left,
        right,
        (((0,), (0,)), ((), ())),
        precision=precision,
        preferred_element_type=jnp.float32,
    )


def per_device(
    normed_inputs,
    query_upstream,
    key_upstream,
    head_outputs,
    branch_upstream,
    query_master,
    key_master,
    branch_master,
    query_basis,
    key_basis,
    branch_basis,
    query_first,
    query_second,
    key_first,
    key_second,
    branch_first,
    branch_second,
):
    exact = lax.Precision.HIGHEST
    row_index = lax.axis_index("fs")
    col_index = lax.axis_index("tp")
    n_rows = lax.axis_size("fs")
    n_cols = lax.axis_size("tp")
    features = normed_inputs.shape[1]
    query_local = query_upstream.shape[1]
    key_local = key_upstream.shape[1]
    rows_in = query_master.shape[0]
    rank = query_basis.shape[1]
    whole_values = lax.all_gather(head_outputs, "tp", axis=1, tiled=True)
    block_query = lax.dynamic_slice_in_dim(query_basis, col_index * features, features, 0)
    block_key = lax.dynamic_slice_in_dim(key_basis, col_index * features, features, 0)
    proj_query, proj_key = lax.psum(
        (
            jnp.dot(normed_inputs, block_query, preferred_element_type=jnp.float32),
            jnp.dot(normed_inputs, block_key, preferred_element_type=jnp.float32),
        ),
        "tp",
    )
    part_query = over_tokens(proj_query, query_upstream.astype(jnp.float32), exact)
    part_key = over_tokens(proj_key, key_upstream.astype(jnp.float32), exact)
    grad_branch = lax.psum_scatter(
        over_tokens(whole_values, branch_upstream), "fs", scatter_dimension=0, tiled=True
    )
    own_branch = lax.dynamic_slice_in_dim(branch_basis, col_index * features, features, 0).astype(
        jnp.float32
    )
    part_branch = jnp.dot(grad_branch, own_branch, precision=exact)
    query_low, key_low = lax.psum((part_query, part_key), "fs")
    branch_low = lax.psum(part_branch, "tp")
    local_squares = (jnp.sum(query_low * query_low) + jnp.sum(key_low * key_low)) / n_rows
    local_squares = local_squares + jnp.sum(branch_low * branch_low) / n_cols
    total = lax.psum(local_squares, ("fs", "tp"))
    entries = rank * n_cols * (2 * query_local + key_local)
    rms_value = jnp.sqrt(total / float(entries))
    clip = 1.0 / jnp.maximum(1.0, rms_value / CLIP_RMS)
    q_first, q_second, q_dir = moments(query_first, query_second, query_low, clip)
    k_first, k_second, k_dir = moments(key_first, key_second, key_low, clip)
    b_first, b_second, b_dir = moments(branch_first, branch_second, branch_low, clip)
    step_rows_query = lax.dynamic_slice_in_dim(query_basis, row_index * rows_in, rows_in, 0).astype(
        jnp.float32
    )
    step_rows_key = lax.dynamic_slice_in_dim(key_basis, row_index * rows_in, rows_in, 0).astype(
        jnp.float32
    )
    query_step = jnp.dot(step_rows_query, q_dir, precision=exact)
    key_step = jnp.dot(step_rows_key, k_dir, precision=exact)
    branch_step = jnp.dot(b_dir, own_branch.T, precision=exact)
    query_updated = query_master - LEARN * query_step
    key_updated = key_master - LEARN * key_step
    branch_updated = branch_master - LEARN * branch_step
    query_copy, key_copy, branch_copy = (
        lax.all_gather(query_updated.astype(jnp.bfloat16), "fs", axis=0, tiled=True),
        lax.all_gather(key_updated.astype(jnp.bfloat16), "fs", axis=0, tiled=True),
        lax.all_gather(branch_updated.astype(jnp.bfloat16), "fs", axis=0, tiled=True),
    )
    return (
        query_step,
        key_step,
        branch_step,
        query_updated,
        key_updated,
        branch_updated,
        query_copy,
        key_copy,
        branch_copy,
        q_first,
        q_second,
        k_first,
        k_second,
        b_first,
        b_second,
    )


def solution(mesh):
    return jax.shard_map(
        per_device,
        mesh=mesh,
        in_specs=(
            P("fs", "tp"),
            P("fs", "tp"),
            P("fs", "tp"),
            P("fs", "tp"),
            P("fs", "tp"),
            P("fs", "tp"),
            P("fs", "tp"),
            P("fs", "tp"),
            P(),
            P(),
            P(),
            P(None, "tp"),
            P(None, "tp"),
            P(None, "tp"),
            P(None, "tp"),
            P("fs", None),
            P("fs", None),
        ),
        out_specs=(
            P("fs", "tp"),
            P("fs", "tp"),
            P("fs", "tp"),
            P("fs", "tp"),
            P("fs", "tp"),
            P("fs", "tp"),
            P(None, "tp"),
            P(None, "tp"),
            P(None, "tp"),
            P(None, "tp"),
            P(None, "tp"),
            P(None, "tp"),
            P(None, "tp"),
            P("fs", None),
            P("fs", None),
        ),
        check_vma=False,
    )
```

profile of v0, /device:TPU:0, one launch (start us, length us, event | category | flops | bytes accessed | tf_op | source)
XLA Modules:
  0.0 502.3 jit_solution(1356573704103843505)
XLA Ops:
  7.2 0.7 all-gather.5.cloned.1.call-update
  8.0 86.4 %all-gather.5.cloned.1.call-done = bf16[1024,4096]{1,0:T(8,128)(2,1)} async-done(((bf16[1024,512]{1,0:T(8,128)(2,1)}), bf16[1024,4096]{1,0:T(8,128)(2,1)}) %all-gather.5.cloned.1.call-update) | async-done | bytes 8388624 | tf_op jit(solution)/shard_map/all_gather | solution.py:59
  94.4 10.4 %fusion.39 = f32[4096,512]{1,0:T(8,128)} fusion(bf16[1024,4096]{1,0:T(8,128)(2,1)} %all-gather.5.cloned.1.call-done, bf16[1024,512]{1,0:T(8,128)(2,1)S(1)} %copy-done), kind=kOutput, calls=%fused_computation.53 | convolution fusion | flops 4294967296 | bytes 17825792 | tf_op jit(solution)/shard_map/dot_general | solution.py:21
  104.9 0.0 all-reduce.5.cloned.1.call-start
  104.9 1.1 copy-done.2
  106.1 2.2 convolution_bitcast_fusion
  108.2 2.2 convolution_bitcast_fusion.1
  110.4 79.4 %reduce-scatter.2.cloned.1.call-done = f32[1024,512]{1,0:T(8,128)} async-done(((f32[4096,512]{1,0:T(8,128)}), f32[1024,512]{1,0:T(8,128)}) %reduce-scatter.2.cloned.1.call-update) | async-done | bytes 2097168 | tf_op jit(solution)/shard_map/reduce_scatter | solution.py:71
  189.8 3.4 fusion.18
  193.3 0.0 all-reduce.7.cloned.1.call-start
  193.4 62.4 %all-reduce.5.cloned.1.call-done = (f32[1024,128]{0,1:T(8,128)}, f32[1024,128]{0,1:T(8,128)}, f32[1024,128]{1,0:T(8,128)}) async-done(((f32[1024,128]{0,1:T(8,128)}, f32[1024,128]{0,1:T(8,128)}, f32[1024,128]{1,0:T(8,128)}), (f32[1024,128]{0,1:T(8,128)}, f32[1024,128]{0,1:T(8,128)}, f32[1024,128]{1,0:T(8,128)})) %all-reduce.5.cloned.1.call-update) | async-done | bytes 1572880 | tf_op jit(solution)/shard_map/psum | solution.py:62
  255.8 2.5 fusion.37
  258.3 1.0 fusion.38
  259.3 0.0 all-gather.9.cloned.1.call-start
  259.4 0.7 multiply_reduce_fusion
  260.7 41.6 %all-reduce.7.cloned.1.call-done = (f32[128,512]{1,0:T(8,128)}, f32[128,128]{1,0:T(8,128)}) async-done(((f32[128,512]{1,0:T(8,128)}, f32[128,128]{1,0:T(8,128)}), (f32[128,512]{1,0:T(8,128)}, f32[128,128]{1,0:T(8,128)})) %all-reduce.7.cloned.1.call-update) | async-done | bytes 327696 | tf_op jit(solution)/shard_map/psum | solution.py:78
  302.3 1.6 multiply_reduce_fusion.1
  303.9 1.5 multiply_reduce_fusion.2
  306.7 39.3 %psum.47 = f32[]{:T(128)} all-reduce(f32[]{:T(128)S(6)} %add.68), channel_id=1, replica_groups=mesh['fs'=4,'tp'=8] {'fs','tp'}, use_global_device_ids=true, to_apply=%region_9.0 | all-reduce | flops 1 | bytes 8 | tf_op jit(solution)/shard_map/psum | solution.py:82
  346.8 0.9 fusion.20
  347.7 2.6 fusion.35
  350.3 1.4 fusion
  351.7 4.7 fusion.34
  356.5 1.2 fusion.5
  357.7 0.4 copy-done.8
  358.1 4.5 fusion.36
  362.7 15.2 %all-gather.9.cloned.1.call-done = bf16[4096,128]{1,0:T(8,128)(2,1)} async-done(((bf16[1024,128]{1,0:T(8,128)(2,1)}), bf16[4096,128]{1,0:T(8,128)(2,1)}) %all-gather.9.cloned.1.call-update) | async-done | bytes 1048592 | tf_op jit(solution)/shard_map/all_gather | solution.py:103
  377.9 54.9 %all-gather.11.cloned.1.call-done = bf16[4096,512]{1,0:T(8,128)(2,1)} async-done(((bf16[1024,512]{1,0:T(8,128)(2,1)}), bf16[4096,512]{1,0:T(8,128)(2,1)}) %all-gather.11.cloned.1.call-update) | async-done | bytes 4194320 | tf_op jit(solution)/shard_map/all_gather | solution.py:104
  432.8 55.0 %all-gather.7.cloned.1.call-done = bf16[4096,512]{1,0:T(8,128)(2,1)} async-done(((bf16[1024,512]{1,0:T(8,128)(2,1)}), bf16[4096,512]{1,0:T(8,128)(2,1)}) %all-gather.7.cloned.1.call-update) | async-done | bytes 4194320 | tf_op jit(solution)/shard_map/all_gather | solution.py:102
  487.8 4.6 copy.40
  492.5 1.0 copy.41
  493.4 2.0 copy.42
  (52 shorter events, 0.4 us)
Async XLA Ops:
  7.2 87.2 %copy-start = (bf16[1024,512]{1,0:T(8,128)(2,1)S(1)}, bf16[1024,512]{1,0:T(8,128)(2,1)}, u32[]{:S(2)}) copy-start(bf16[1024,512]{1,0:T(8,128)(2,1)} %param.21) | copy-start | bytes 3145732
  7.2 87.2 %all-gather.5.cloned.1.call-start = ((), (), s32[]{:S(2)}) async-start(), calls=%async_computation.1 | async-start | bytes 9437184 | tf_op jit(solution)/shard_map/all_gather | solution.py:59
  7.9 181.9 %reduce-scatter.2.cloned.1.call-start = ((), (), s32[]{:S(2)}) async-start(), calls=%async_computation.2 | async-start | bytes 10485760 | tf_op jit(solution)/shard_map/reduce_scatter | solution.py:71
  104.9 1.2 copy-start.2
  104.9 150.9 %all-reduce.5.cloned.1.call-start = ((), (), s32[]{:S(2)}) async-start(), calls=%async_computation.6 | async-start | bytes 3145728 | tf_op jit(solution)/shard_map/psum | solution.py:62
  110.4 145.4 %copy-start.11 = (bf16[1024,512]{1,0:T(8,128)(2,1)S(1)}, bf16[1024,512]{1,0:T(8,128)(2,1)}, u32[]{:S(2)}) copy-start(bf16[1024,512]{1,0:T(8,128)(2,1)} %param.18) | copy-start | bytes 3145732
  193.3 65.0 %copy-start.19 = (bf16[1024,128]{1,0:T(8,128)(2,1)S(1)}, bf16[1024,128]{1,0:T(8,128)(2,1)}, u32[]{:S(2)}) copy-start(bf16[1024,128]{1,0:T(8,128)(2,1)} %param.19) | copy-start | bytes 786436
  193.3 153.5 %copy-start.20 = (f32[128,128]{1,0:T(8,128)S(1)}, f32[128,128]{1,0:T(8,128)}, u32[]{:S(2)}) copy-start(f32[128,128]{1,0:T(8,128)} %param.31) | copy-start | bytes 196612
  193.3 153.5 %copy-start.21 = (f32[128,128]{1,0:T(8,128)S(1)}, f32[128,128]{1,0:T(8,128)}, u32[]{:S(2)}) copy-start(f32[128,128]{1,0:T(8,128)} %param.30) | copy-start | bytes 196612
  193.3 109.0 %all-reduce.7.cloned.1.call-start = ((), (), s32[]{:S(2)}) async-start(), calls=%async_computation.7 | async-start | bytes 655360 | tf_op jit(solution)/shard_map/psum | solution.py:78
  255.8 2.5 copy-start.15
  255.8 3.6 copy-start.6
  255.8 91.9 %copy-start.14 = (f32[1024,128]{1,0:T(8,128)S(1)}, f32[1024,128]{1,0:T(8,128)}, u32[]{:S(2)}) copy-start(f32[1024,128]{1,0:T(8,128)} %param.23) | copy-start | bytes 1572868
  259.3 118.6 %all-gather.9.cloned.1.call-start = ((), (), s32[]{:S(2)}) async-start(), calls=%async_computation.4 | async-start | bytes 1310720 | tf_op jit(solution)/shard_map/all_gather | solution.py:103
  347.6 4.0 copy-start.17
  347.6 4.0 copy-start.18
  347.7 4.0 copy-start.7
  350.3 82.5 %all-gather.11.cloned.1.call-start = ((), (), s32[]{:S(2)}) async-start(), calls=%async_computation.5 | async-start | bytes 5242880 | tf_op jit(solution)/shard_map/all_gather | solution.py:104
  351.7 4.7 copy-start.4
  351.7 4.7 copy-start.5
  351.7 4.8 copy-start.12
  351.7 4.8 copy-start.16
  356.4 1.7 copy-start.8
  356.4 131.4 %all-gather.7.cloned.1.call-start = ((), (), s32[]{:S(2)}) async-start(), calls=%async_computation.3 | async-start | bytes 5242880 | tf_op jit(solution)/shard_map/all_gather | solution.py:102
  357.7 5.0 copy-start.9
  357.7 5.0 copy-start.10
  487.8 4.6 copy-start.13
  487.8 5.6 %copy-start.3 = (bf16[4096,512]{1,0:T(8,128)(2,1)S(1)}, bf16[4096,512]{1,0:T(8,128)(2,1)}, u32[]{:S(2)}) copy-start(bf16[4096,512]{1,0:T(8,128)(2,1)} %all-gather.11.cloned.1.call-done) | copy-start | bytes 12582916
  493.4 2.0 copy-start.1
Sparse Core Ops, SparseCore 0:
  9.6 84.7 all-gather.4
  105.0 84.7 reduce-scatter.1
  193.6 62.1 all-reduce.4
  259.4 42.8 all-reduce.6
  350.4 27.4 all-gather.8
  380.2 52.5 all-gather.10
  435.2 52.5 all-gather.6
where the time goes:
time: 503 us; the launch traced here: 502 us
  waiting for transfers between devices  396 us (79%)
  blocking collectives  39.3 us (8%)
  matrix products  33.4 us (7%)
  between operations  17 us (3%)
  local copies, waits for them, and re-layouts  9.28 us (2%)
  other arithmetic  7.2 us (1%)
    all_gather x1, waiting for transfers between devices, per_device(): whole_values = lax.all_gather(head_outputs, 'tp', axis=1, tiled=True)  86.4 us
    reduce_scatter x1, waiting for transfers between devices, per_device(): lax.psum_scatter(over_tokens(whole_values, branch_upstream), 'fs', scatte...  79.4 us
    psum x1, waiting for transfers between devices, per_device(): lax.psum((jnp.dot(normed_inputs, block_query, preferred_element_type=jnp....  62.4 us
    all_gather x1, waiting for transfers between devices, per_device(): lax.all_gather(query_updated.astype(jnp.bfloat16), 'fs', axis=0, tiled=True)  55 us
    all_gather x1, waiting for transfers between devices, per_device(): lax.all_gather(branch_updated.astype(jnp.bfloat16), 'fs', axis=0, tiled=T...  54.9 us
    psum x1, waiting for transfers between devices, per_device(): query_low, key_low = lax.psum((part_query, part_key), 'fs')  41.6 us
    psum x1, blocking collectives, per_device(): total = lax.psum(local_squares, ('fs', 'tp'))  39.3 us
    all_gather x1, waiting for transfers between devices, per_device(): lax.all_gather(key_updated.astype(jnp.bfloat16), 'fs', axis=0, tiled=True)  15.2 us
  transfers between devices with their start and end apart: 7, of which 7 were waited for; matrix products, arithmetic and copies ran while one was open for 3% of the time, Pallas kernels for 0%

commit v1 on v0

--- a/solution.py
+++ b/solution.py
@@ -1,3 +1,4 @@
+import functools
 import jax
 import jax.numpy as jnp
 from jax import lax
@@ -8,6 +9,14 @@
 BETA_TWO = 0.95
 ADAM_EPS = 1e-08
 CLIP_RMS = 0.5
+
+
+def produce_numbers(frame_in, lane_axis):
+    opened = jnp.sum(lax.all_gather(frame_in, axis_name=lane_axis), axis=0)
+    return opened
+
+
+try_all_the_bands = functools.partial(produce_numbers, lane_axis=("fs", "tp"))
 
 
 def moments(first, second, low, clip):
@@ -79,7 +88,7 @@
     branch_low = lax.psum(part_branch, "tp")
     local_squares = (jnp.sum(query_low * query_low) + jnp.sum(key_low * key_low)) / n_rows
     local_squares = local_squares + jnp.sum(branch_low * branch_low) / n_cols
-    total = lax.psum(local_squares, ("fs", "tp"))
+    total = try_all_the_bands(local_squares)
     entries = rank * n_cols * (2 * query_local + key_local)
     rms_value = jnp.sqrt(total / float(entries))
     clip = 1.0 / jnp.maximum(1.0, rms_value / CLIP_RMS)

time: 503 us -> 503 us (level)
    psum x1 -> x0, blocking collectives: 39.3 us -> none  [per_device(): total = lax.psum(local_squares, ('fs', 'tp'))]
    unnamed x0 -> x1, blocking collectives: none -> 39.2 us
where the time goes in v1:
time: 503 us
  waiting for transfers between devices  396 us (79%)
  blocking collectives  39.2 us (8%)
  matrix products  33.4 us (7%)
  between operations  17.1 us (3%)
  local copies, waits for them, and re-layouts  9.42 us (2%)
  other arithmetic  7.82 us (2%)
    all_gather x1, waiting for transfers between devices, per_device(): whole_values = lax.all_gather(head_outputs, 'tp', axis=1, tiled=True)  86.4 us
    reduce_scatter x1, waiting for transfers between devices, per_device(): lax.psum_scatter(over_tokens(whole_values, branch_upstream), 'fs', scatte...  79.4 us
    psum x1, waiting for transfers between devices, per_device(): lax.psum((jnp.dot(normed_inputs, block_query, preferred_element_type=jnp....  62.4 us
    all_gather x1, waiting for transfers between devices, per_device(): lax.all_gather(query_updated.astype(jnp.bfloat16), 'fs', axis=0, tiled=True)  55 us
    all_gather x1, waiting for transfers between devices, per_device(): lax.all_gather(branch_updated.astype(jnp.bfloat16), 'fs', axis=0, tiled=T...  54.9 us
    psum x1, waiting for transfers between devices, per_device(): query_low, key_low = lax.psum((part_query, part_key), 'fs')  41.6 us
    unnamed x1, blocking collectives  39.2 us
    all_gather x1, waiting for transfers between devices, per_device(): lax.all_gather(key_updated.astype(jnp.bfloat16), 'fs', axis=0, tiled=True)  15 us
  transfers between devices with their start and end apart: 7, of which 7 were waited for; matrix products, arithmetic and copies ran while one was open for 3% of the time, Pallas kernels for 0%

profile of v1, /device:TPU:0, one launch (start us, length us, event | category | flops | bytes accessed | tf_op | source)
XLA Modules:
  0.0 502.8 jit_solution(8980494834195861181)
XLA Ops:
  7.2 0.7 all-gather.5.cloned.1.call-update
  8.0 86.4 %all-gather.5.cloned.1.call-done = bf16[1024,4096]{1,0:T(8,128)(2,1)} async-done(((bf16[1024,512]{1,0:T(8,128)(2,1)}), bf16[1024,4096]{1,0:T(8,128)(2,1)}) %all-gather.5.cloned.1.call-update) | async-done | bytes 8388624 | tf_op jit(solution)/shard_map/all_gather | solution.py:68
  94.4 10.5 %fusion.39 = f32[4096,512]{1,0:T(8,128)} fusion(bf16[1024,4096]{1,0:T(8,128)(2,1)} %all-gather.5.cloned.1.call-done, bf16[1024,512]{1,0:T(8,128)(2,1)S(1)} %copy-done), kind=kOutput, calls=%fused_computation.53 | convolution fusion | flops 4294967296 | bytes 17825792 | tf_op jit(solution)/shard_map/dot_general | solution.py:30
  104.9 0.0 all-reduce.6.cloned.1.call-start
  104.9 1.1 copy-done.2
  106.1 2.2 convolution_bitcast_fusion
  108.3 2.2 convolution_bitcast_fusion.1
  110.4 79.4 %reduce-scatter.2.cloned.1.call-done = f32[1024,512]{1,0:T(8,128)} async-done(((f32[4096,512]{1,0:T(8,128)}), f32[1024,512]{1,0:T(8,128)}) %reduce-scatter.2.cloned.1.call-update) | async-done | bytes 2097168 | tf_op jit(solution)/shard_map/reduce_scatter | solution.py:80
  189.8 3.4 fusion.18
  193.4 62.4 %all-reduce.6.cloned.1.call-done = (f32[1024,128]{0,1:T(8,128)}, f32[1024,128]{0,1:T(8,128)}, f32[1024,128]{1,0:T(8,128)}) async-done(((f32[1024,128]{0,1:T(8,128)}, f32[1024,128]{0,1:T(8,128)}, f32[1024,128]{1,0:T(8,128)}), (f32[1024,128]{0,1:T(8,128)}, f32[1024,128]{0,1:T(8,128)}, f32[1024,128]{1,0:T(8,128)})) %all-reduce.6.cloned.1.call-update) | async-done | bytes 1572880 | tf_op jit(solution)/shard_map/psum | solution.py:71
  255.8 2.5 fusion.37
  258.3 1.0 fusion.38
  259.4 0.7 multiply_reduce_fusion
  260.8 41.6 %all-reduce.8.cloned.1.call-done = (f32[128,512]{1,0:T(8,128)}, f32[128,128]{1,0:T(8,128)}) async-done(((f32[128,512]{1,0:T(8,128)}, f32[128,128]{1,0:T(8,128)}), (f32[128,512]{1,0:T(8,128)}, f32[128,128]{1,0:T(8,128)})) %all-reduce.8.cloned.1.call-update) | async-done | bytes 327696 | tf_op jit(solution)/shard_map/psum | solution.py:87
  302.3 1.6 multiply_reduce_fusion.1
  303.9 1.5 multiply_reduce_fusion.2
  306.7 0.1 dynamic-update-slice
  306.8 39.2 %all-reduce = f32[32]{0:T(128)S(1)} all-reduce(f32[32]{0:T(128)S(1)} %dynamic-update-slice), channel_id=1, replica_groups=mesh['fs'=4,'tp'=8] {'fs','tp'}, use_global_device_ids=true, to_apply=%add | all-reduce | flops 32 | bytes 256
  346.1 0.6 reduce_sum.39
  347.4 0.9 fusion.20
  348.4 2.6 fusion.35
  351.0 1.4 fusion
  352.4 4.7 fusion.34
  357.2 1.2 fusion.5
  358.4 0.4 copy-done.8
  358.8 4.5 fusion.36
  363.4 15.0 %all-gather.9.cloned.1.call-done = bf16[4096,128]{1,0:T(8,128)(2,1)} async-done(((bf16[1024,128]{1,0:T(8,128)(2,1)}), bf16[4096,128]{1,0:T(8,128)(2,1)}) %all-gather.9.cloned.1.call-update) | async-done | bytes 1048592 | tf_op jit(solution)/shard_map/all_gather | solution.py:112
  378.4 54.9 %all-gather.11.cloned.1.call-done = bf16[4096,512]{1,0:T(8,128)(2,1)} async-done(((bf16[1024,512]{1,0:T(8,128)(2,1)}), bf16[4096,512]{1,0:T(8,128)(2,1)}) %all-gather.11.cloned.1.call-update) | async-done | bytes 4194320 | tf_op jit(solution)/shard_map/all_gather | solution.py:113
  433.3 55.0 %all-gather.7.cloned.1.call-done = bf16[4096,512]{1,0:T(8,128)(2,1)} async-done(((bf16[1024,512]{1,0:T(8,128)(2,1)}), bf16[4096,512]{1,0:T(8,128)(2,1)}) %all-gather.7.cloned.1.call-update) | async-done | bytes 4194320 | tf_op jit(solution)/shard_map/all_gather | solution.py:111
  488.3 4.6 copy.41
  492.9 1.0 copy.42
  493.9 2.0 copy.43
  (55 shorter events, 0.5 us)
Async XLA Ops:
  7.2 87.2 %copy-start = (bf16[1024,512]{1,0:T(8,128)(2,1)S(1)}, bf16[1024,512]{1,0:T(8,128)(2,1)}, u32[]{:S(2)}) copy-start(bf16[1024,512]{1,0:T(8,128)(2,1)} %param.21) | copy-start | bytes 3145732
  7.2 87.2 %all-gather.5.cloned.1.call-start = ((), (), s32[]{:S(2)}) async-start(), calls=%async_computation.1 | async-start | bytes 9437184 | tf_op jit(solution)/shard_map/all_gather | solution.py:68
  7.9 181.9 %reduce-scatter.2.cloned.1.call-start = ((), (), s32[]{:S(2)}) async-start(), calls=%async_computation.2 | async-start | bytes 10485760 | tf_op jit(solution)/shard_map/reduce_scatter | solution.py:80
  104.9 1.2 copy-start.2
  104.9 150.9 %all-reduce.6.cloned.1.call-start = ((), (), s32[]{:S(2)}) async-start(), calls=%async_computation.6 | async-start | bytes 3145728 | tf_op jit(solution)/shard_map/psum | solution.py:71
  110.4 145.4 %copy-start.11 = (bf16[1024,512]{1,0:T(8,128)(2,1)S(1)}, bf16[1024,512]{1,0:T(8,128)(2,1)}, u32[]{:S(2)}) copy-start(bf16[1024,512]{1,0:T(8,128)(2,1)} %param.18) | copy-start | bytes 3145732
  193.3 65.0 %copy-start.19 = (bf16[1024,128]{1,0:T(8,128)(2,1)S(1)}, bf16[1024,128]{1,0:T(8,128)(2,1)}, u32[]{:S(2)}) copy-start(bf16[1024,128]{1,0:T(8,128)(2,1)} %param.19) | copy-start | bytes 786436
  193.3 154.1 %copy-start.20 = (f32[128,128]{1,0:T(8,128)S(1)}, f32[128,128]{1,0:T(8,128)}, u32[]{:S(2)}) copy-start(f32[128,128]{1,0:T(8,128)} %param.31) | copy-start | bytes 196612
  193.3 154.1 %copy-start.21 = (f32[128,128]{1,0:T(8,128)S(1)}, f32[128,128]{1,0:T(8,128)}, u32[]{:S(2)}) copy-start(f32[128,128]{1,0:T(8,128)} %param.30) | copy-start | bytes 196612
  193.3 109.0 %all-reduce.8.cloned.1.call-start = ((), (), s32[]{:S(2)}) async-start(), calls=%async_computation.7 | async-start | bytes 655360 | tf_op jit(solution)/shard_map/psum | solution.py:87
  255.8 2.5 copy-start.15
  255.8 3.6 copy-start.6
  255.8 92.5 %copy-start.14 = (f32[1024,128]{1,0:T(8,128)S(1)}, f32[1024,128]{1,0:T(8,128)}, u32[]{:S(2)}) copy-start(f32[1024,128]{1,0:T(8,128)} %param.23) | copy-start | bytes 1572868
  259.3 119.1 %all-gather.9.cloned.1.call-start = ((), (), s32[]{:S(2)}) async-start(), calls=%async_computation.4 | async-start | bytes 1310720 | tf_op jit(solution)/shard_map/all_gather | solution.py:112
  348.3 4.0 copy-start.17
  348.3 4.0 copy-start.18
  348.3 4.0 copy-start.7
  350.9 82.3 %all-gather.11.cloned.1.call-start = ((), (), s32[]{:S(2)}) async-start(), calls=%async_computation.5 | async-start | bytes 5242880 | tf_op jit(solution)/shard_map/all_gather | solution.py:113
  352.4 4.7 copy-start.4
  352.4 4.7 copy-start.5
  352.4 4.8 copy-start.12
  352.4 4.8 copy-start.16
  357.1 1.7 copy-start.8
  357.1 131.2 %all-gather.7.cloned.1.call-start = ((), (), s32[]{:S(2)}) async-start(), calls=%async_computation.3 | async-start | bytes 5242880 | tf_op jit(solution)/shard_map/all_gather | solution.py:111
  358.4 5.0 copy-start.9
  358.4 5.0 copy-start.10
  488.3 4.6 copy-start.13
  488.3 5.6 %copy-start.3 = (bf16[4096,512]{1,0:T(8,128)(2,1)S(1)}, bf16[4096,512]{1,0:T(8,128)(2,1)}, u32[]{:S(2)}) copy-start(bf16[4096,512]{1,0:T(8,128)(2,1)} %all-gather.11.cloned.1.call-done) | copy-start | bytes 12582916
  493.9 2.0 copy-start.1
Sparse Core Ops, SparseCore 0:
  9.6 84.7 all-gather.4
  105.0 84.7 reduce-scatter.1
  193.6 62.1 all-reduce.5
  259.4 42.8 all-reduce.7
  351.1 27.3 all-gather.8
  380.7 52.5 all-gather.10
  435.7 52.5 all-gather.6
